TPU v7x, 32 devices: a whole 2x2x4 slice. The times are simulated.
32 devices in a mesh: grp: 2 (over y), sp: 4 (over z), tp: 4 (over x, core).
Axes of the slice: x: 2, y: 2, z: 4, core: 2. Of those that a mesh axis runs over, the one named last changes fastest.
Arguments:
- conv_input: bfloat16 [4096, 1024], P(('grp', 'sp'), 'tp'), parts along dimension 0, may hold values from -6 to 6
- pre_gate: bfloat16 [4096, 1024], P(('grp', 'sp'), 'tp'), parts along dimension 0, may hold values from -6 to 6
- post_gate: bfloat16 [4096, 1024], P(('grp', 'sp'), 'tp'), parts along dimension 0, may hold values from -6 to 6
- conv_taps: float32 [3, 1024], replicated, may hold values from -3.5 to 3.5
- out_proj: bfloat16 [1024, 2048], replicated, may hold values from -0.1875 to 0.1875
- residual_in: bfloat16 [4096, 2048], P(('grp', 'sp', 'tp')), parts along dimension 0, may hold values from -6 to 6
- norm_gain: float32 [2048], replicated, may hold values from 0.1 to 1.9
- routes: int32 [4096, 2], P(('grp', 'sp', 'tp')), parts along dimension 0, may hold values from 0 to 7, as said below
- route_weight: float32 [4096, 2], P(('grp', 'sp', 'tp')), parts along dimension 0, may hold values from 0.1 to 1
- w_gate: bfloat16 [8, 2048, 1024], P('sp', None, 'tp'), may hold values from -0.125 to 0.125
- w_up: bfloat16 [8, 2048, 1024], P('sp', None, 'tp'), may hold values from -0.125 to 0.125
- w_down: bfloat16 [8, 1024, 2048], P('sp', 'tp'), may hold values from -0.1875 to 0.1875
Outputs:
- layer_out: bfloat16 [4096, 2048], P(('grp', 'sp', 'tp')), parts along dimension 0
There are 2 independent parts, one for each index of `grp`. A program takes and returns all parts, laid end to end along the dimension named above; an argument that names none is the same for every part. Nothing has to cross between parts.
Inputs may be any that keep to these rules, and one draw needn't show every extreme that they name: `routes`: the two numbers of a row differ and lie in the same group of 2 consecutive experts. In each aligned block of 128 rows every expert is named exactly 32 times.
All inputs are finite; a program needn't handle non-finite values.
Results may differ from a plain program's by a relative error of at most 0.0085.
Values may be sent and summed in bfloat16 or wider, within the bound.
A program may use at most 64 MiB of HBM per device.

v0:
```python
import functools

import jax
import jax.numpy as jnp
from jax import lax
from jax.experimental import pallas as pl
from jax.experimental.pallas import tpu as pltpu
from jax.sharding import PartitionSpec as P

GROUPS = 4
LANES = 128
F32, BF16 = jnp.float32, jnp.bfloat16


def shifted(block, axis, distance):
    devices = range(lax.axis_size(axis))
    route = [(i - distance, i) for i in devices if i - distance in devices]
    return lax.ppermute(block, axis, route)


def generic(
    conv_input,
    pre_gate,
    post_gate,
    conv_taps,
    out_proj,
    residual_in,
    norm_gain,
    routes,
    route_weight,
    w_gate,
    w_up,
    w_down,
):
    shards = lax.axis_size("tp")
    place = lax.axis_index("tp")
    seq_ranks = lax.axis_size("sp")
    channels = conv_input.shape[1]
    width = residual_in.shape[1]
    taps = lax.dynamic_slice_in_dim(conv_taps, place * channels, channels, 1)
    prior_input, prior_gate = shifted((conv_input[-2:], pre_gate[-2:]), "sp", 1)
    gated = jnp.concatenate(
        [
            prior_gate.astype(jnp.float32) * prior_input.astype(jnp.float32),
            pre_gate.astype(jnp.float32) * conv_input.astype(jnp.float32),
        ],
        axis=0,
    )
    conv = gated[2:] * taps[2] + gated[1:-1] * taps[1] + gated[:-2] * taps[0]
    mixed = (post_gate.astype(jnp.float32) * conv).astype(jnp.bfloat16)
    token_rows = lax.all_to_all(mixed, "tp", split_axis=0, concat_axis=1, tiled=True)
    projected = jnp.dot(token_rows, out_proj, preferred_element_type=jnp.float32)
    stream = residual_in.astype(jnp.float32) + projected
    scale = lax.rsqrt(jnp.mean(stream * stream, axis=-1, keepdims=True) + 1e-06)
    normed = (stream * scale * norm_gain).astype(jnp.bfloat16)
    block_rows = routes.shape[0]
    local_experts = w_gate.shape[0]
    experts = local_experts * seq_ranks
    capacity = 2 * block_rows // experts
    flat_routes = routes.reshape(-1)
    position = jnp.arange(flat_routes.shape[0], dtype=jnp.int32)
    earlier = (flat_routes[:, None] == flat_routes[None, :]) & (
        position[None, :] < position[:, None]
    )
    rank = jnp.sum(earlier.astype(jnp.int32), axis=1)
    slot = flat_routes * capacity + rank
    outgoing = (
        jnp.zeros((experts * capacity, width), jnp.bfloat16).at[slot].set(normed[position // 2])
    )
    outgoing = outgoing.reshape(seq_ranks, local_experts, capacity, width)
    spread = lax.all_gather(
        lax.all_to_all(outgoing, "sp", split_axis=0, concat_axis=0, tiled=True)[:, None],
        "tp",
        axis=1,
        tiled=True,
    )
    count = spread.shape[3]
    partials = []
    for expert in range(local_experts):
        rows = spread[:, :, expert].reshape(seq_ranks * shards * count, width)
        gate = jnp.dot(rows, w_gate[expert], preferred_element_type=jnp.float32)
        upper = jnp.dot(rows, w_up[expert], preferred_element_type=jnp.float32)
        hidden = (jax.nn.silu(gate) * upper).astype(jnp.bfloat16)
        part = jnp.dot(hidden, w_down[expert], preferred_element_type=jnp.float32).astype(
            jnp.bfloat16
        )
        partials.append(part.reshape(seq_ranks, shards, count, width))
    stacked = jnp.stack(partials, axis=2)
    summed = lax.psum_scatter(stacked, "tp", scatter_dimension=1, tiled=True).astype(jnp.float32)
    returned = lax.all_to_all(
        summed[:, 0].astype(jnp.bfloat16), "sp", split_axis=0, concat_axis=0, tiled=True
    )
    results = returned.reshape(experts * capacity, width)[slot]
    results = results.reshape(block_rows, 2, width).astype(jnp.float32)
    weighted = jnp.sum(route_weight[:, :, None] * results, axis=1)
    return (stream + weighted).astype(jnp.bfloat16)


def dot(a, b):
    return jnp.dot(a, b, preferred_element_type=F32)


def fused_kernel(
    input_hbm,
    pre_hbm,
    post_hbm,
    conv_taps,
    proj_hbm,
    residual_hbm,
    gain,
    routes,
    route_weight,
    gate_hbm,
    up_hbm,
    down_hbm,
    out,
    conv_input,
    pre_gate,
    post_gate,
    residual,
    proj,
    w_gate,
    w_up,
    w_down,
    halo,
    gated,
    mix_out,
    mix_in,
    stream,
    leaving,
    tok,
    hidden,
    part,
    from_core,
    kept,
    to_chip,
    from_chip,
    to_home,
    home,
    load_sem,
    halo_send,
    halo_recv,
    mix_send,
    mix_recv,
    z_send,
    z_recv,
    x_send,
    x_recv,
    c_send,
    c_recv,
    d_send,
    d_recv,
    one_send,
    one_recv,
    two_send,
    two_recv,
    home_send,
    home_recv,
):
    s, t = lax.axis_index("sp"), lax.axis_index("tp")
    rows, width = residual.shape
    channels = conv_input.shape[1]
    cap = rows // GROUPS
    units = w_gate.shape[2]
    core, chip, far = t + 1 - 2 * (t % 2), (t + 2) % 4, 3 - t
    sp_of = [s, s + 1 - 2 * (s % 2), (s + 2) % 4, 3 - s]
    pos = lambda place: (place % 2) * 2 + place // 2
    pending = []

    def send(src, dst, send_sem, recv_sem, **where):
        copy = pltpu.make_async_remote_copy(
            src_ref=src,
            dst_ref=dst,
            send_sem=send_sem,
            recv_sem=recv_sem,
            device_id=where,
            device_id_type=pl.DeviceIdType.MESH,
        )
        copy.start()
        pending.append(copy)
        return copy

    barrier = pltpu.get_barrier_semaphore()
    for other in (core, chip, far):
        pl.semaphore_signal(
            barrier, inc=1, device_id={"tp": other}, device_id_type=pl.DeviceIdType.MESH
        )
    for other in sp_of[1:]:
        pl.semaphore_signal(
            barrier, inc=1, device_id={"sp": other}, device_id_type=pl.DeviceIdType.MESH
        )
    loads = []
    for i, (a, b) in enumerate(
        (
            (input_hbm, conv_input),
            (pre_hbm, pre_gate),
            (post_hbm, post_gate),
            (residual_hbm, residual),
            (proj_hbm, proj),
            (gate_hbm, w_gate),
            (up_hbm, w_up),
            (down_hbm, w_down),
        )
    ):
        loads.append(pltpu.make_async_copy(a, b, load_sem.at[i]))
        loads[-1].start()

    first, second = routes[0:1, :], routes[1:2, :]
    epg = w_gate.shape[0]
    down = lax.broadcasted_iota(jnp.int32, (rows, rows), 0)
    across = lax.broadcasted_iota(jnp.int32, (rows, rows), 1)
    group = lax.broadcasted_iota(jnp.int32, (16, rows), 0)
    member = (first >= group * epg) & (first < group * epg + epg) & (group < GROUPS)
    member = jnp.where(member, 1.0, 0.0)
    earlier = jnp.where(down < across, 1.0, 0.0).astype(BF16)
    rank = dot(member.astype(BF16), earlier)
    slot = jnp.sum(member * (rank + (group * cap).astype(F32)), axis=0, keepdims=True)
    pick = jnp.where(slot == down.astype(F32), 1.0, 0.0)
    back = pick.T.astype(BF16)
    pick = pick.astype(BF16)
    low = jnp.where(first < second, route_weight[0:1, :], route_weight[1:2, :])
    high = jnp.where(first < second, route_weight[1:2, :], route_weight[0:1, :])
    low_top, high_top = low.astype(BF16).astype(F32), high.astype(BF16).astype(F32)
    line = lax.broadcasted_iota(jnp.int32, (LANES, rows), 0)
    scales = jnp.where(
        line == 0,
        low_top,
        jnp.where(
            line == 1,
            low - low_top,
            jnp.where(line == 2, high_top, jnp.where(line == 3, high - high_top, 0.0)),
        ),
    ).astype(BF16)
    scales = lax.dot_general(
        pick, scales, (((1,), (1,)), ((), ())), preferred_element_type=F32
    )
    leaving[:, pl.ds(width, LANES)] = scales.astype(BF16)

    loads[0].wait()
    loads[1].wait()
    pl.semaphore_wait(barrier, 6)

    count = conv_input.shape[0]
    halo_copies = [
        send(
            ref.at[pl.ds(count - 16, 16), :],
            halo.at[i],
            halo_send.at[i],
            halo_recv.at[i],
            sp=(s + 1) % 4,
        )
        for i, ref in enumerate((conv_input, pre_gate))
    ]
    gated[pl.ds(8, count), :] = pre_gate[...].astype(F32) * conv_input[...].astype(F32)
    taps = conv_taps[:, pl.ds(pl.multiple_of(t * channels, channels), channels)]
    loads[2].wait()

    def mix(place):
        start = pl.multiple_of(place * rows, rows)
        g = gated[pl.ds(start, rows + 8), :]
        conv = g[8:] * taps[2:3] + g[7:-1] * taps[1:2] + g[6:-2] * taps[0:1]
        return (post_gate[pl.ds(start, rows), :].astype(F32) * conv).astype(BF16)

    def send_mixed(i, place):
        mix_out[i] = mix(place)
        send(mix_out.at[i], mix_in.at[t], mix_send.at[i], mix_recv.at[t], tp=place)

    def wait_mixed(place):
        pltpu.make_async_remote_copy(
            src_ref=mix_in.at[place],
            dst_ref=mix_in.at[place],
            send_sem=mix_send.at[0],
            recv_sem=mix_recv.at[place],
            device_id={"tp": place},
            device_id_type=pl.DeviceIdType.MESH,
        ).wait_recv()

    across_chip = 2 * (1 - t // 2)
    send_mixed(0, across_chip + 1)
    for copy in halo_copies:
        copy.wait_recv()
    before = halo[0, 8:16, :].astype(F32) * halo[1, 8:16, :].astype(F32)
    gated[0:8, :] = jnp.where(s > 0, before, 0.0)
    send_mixed(1, across_chip)
    send_mixed(2, core)
    mix_in[t] = mix(t)

    tile = 512
    tiles = width // tile
    column = lambda n: pl.ds(pl.multiple_of(n * tile, tile), tile)
    weights_of = lambda place: pl.ds(pl.multiple_of(place * channels, channels), channels)
    loads[3].wait()
    loads[4].wait()
    wait_mixed(core)

    def project_near(n, carry):
        cols = column(n)
        total = residual[:, cols].astype(F32)
        for place in (t, core):
            total += dot(mix_in[place], proj[weights_of(place), cols])
        stream[:, cols] = total
        return carry

    lax.fori_loop(0, tiles, project_near, 0)
    wait_mixed(chip)
    wait_mixed(far)

    def project_far(n, squares):
        cols = column(n)
        total = stream[:, cols]
        for place in (chip, far):
            total += dot(mix_in[place], proj[weights_of(place), cols])
        stream[:, cols] = total
        return squares + jnp.sum(total * total, axis=1, keepdims=True)

    squares = lax.fori_loop(0, tiles, project_far, jnp.zeros((rows, 1), F32))
    scale = lax.rsqrt(squares / width + 1e-06)

    def norm(n, carry):
        cols = column(n)
        row = (stream[:, cols] * scale * gain[:, cols]).astype(BF16)
        leaving[:, cols] = dot(pick, row).astype(BF16)
        return carry

    lax.fori_loop(0, tiles, norm, 0)

    some = cap // 2
    group_rows = lambda g: pl.ds(pl.multiple_of(g * cap, cap), cap)
    part_rows = lambda g, h: pl.ds(pl.multiple_of(g * cap + h * some, some), some)
    block = lambda place: pl.ds(pl.multiple_of(pos(place) * some, some), some)
    z_copies, x_copies, c_copies, d_copies = {}, {}, {}, {}
    one_copies, two_copies, home_copies = {}, {}, {}

    def forward(k, h):
        src = leaving.at[part_rows(s, h), :]
        if k:
            z_copies[k, h].wait_recv()
            src = tok.at[sp_of[k], h, block(t), :]
        dst = tok.at[sp_of[k], h, block(t), :]
        i = 2 * k + h
        x_copies[k, h] = send(src, dst, x_send.at[i], x_recv.at[i], tp=chip)
        c_copies[k, h] = send(src, dst, c_send.at[i], c_recv.at[i], tp=core)

    def pass_on(k, h):
        x_copies[k, h].wait_recv()
        i = 2 * k + h
        arrived = tok.at[sp_of[k], h, block(chip), :]
        d_copies[k, h] = send(arrived, arrived, d_send.at[i], d_recv.at[i], tp=core)

    for k, h in ((1, 0), (1, 1), (2, 0), (2, 1), (3, 0), (3, 1)):
        i = 2 * k + h
        z_copies[k, h] = send(
            leaving.at[part_rows(sp_of[k], h), :],
            tok.at[s, h, block(t), :],
            z_send.at[i],
            z_recv.at[i],
            sp=sp_of[k],
        )
    for h in (0, 1):
        forward(0, h)
        tok[s, h, block(t), :] = leaving[part_rows(s, h), :]
    for load in loads[5:]:
        load.wait()

    def experts(k, *one):
        own = one or (0, 1)
        for h in own:
            c_copies[k, h].wait_recv()
            d_copies[k, h].wait_recv()
        g, low_half, m = sp_of[k], own[0], len(own)
        where, length = pl.ds(low_half, m), m * 2 * cap
        x = tok[g, where, :, 0:width].reshape(length, width)
        top = tok[g, where, :, pl.ds(width, LANES)].reshape(length, LANES).astype(F32)
        for e in range(epg):
            w = top[:, 2 * e : 2 * e + 1] + top[:, 2 * e + 1 : 2 * e + 2]
            gate = dot(x, w_gate[e])
            upper = dot(x, w_up[e])
            act = gate / (1.0 + jnp.exp(-gate)) * upper * w
            hidden[0:length, pl.ds(e * units, units)] = act.astype(BF16)

        def lower(n, carry):
            cols = column(n)
            rows_out = dot(hidden[0:length, :], w_down[:, cols]).astype(BF16)
            part[k, where, :, cols] = rows_out.reshape(m, 2 * cap, tile)
            return carry

        lax.fori_loop(0, tiles, lower, 0)
        for h in own:
            i = 2 * k + h
            one_copies[k, h] = send(
                part.at[k, h, core_rows(1 - t % 2), :],
                from_core.at[k, h],
                one_send.at[i],
                one_recv.at[i],
                tp=core,
            )

    core_rows = lambda c: pl.ds(pl.multiple_of(c * cap, cap), cap)

    def add_core(k, h):
        one_copies[k, h].wait_recv()
        i = 2 * k + h
        for mine in (False, True):
            x = t // 2 if mine else 1 - t // 2
            base = pl.multiple_of((t % 2) * cap + x * some, some)
            near = pl.multiple_of(x * some, some)
            total = part[k, h, pl.ds(base, some), :].astype(F32)
            total += from_core[k, h, pl.ds(near, some), :].astype(F32)
            if mine:
                kept[k, h] = total
            else:
                to_chip[k, h] = total.astype(BF16)
                two_copies[k, h] = send(
                    to_chip.at[k, h],
                    from_chip.at[k, h],
                    two_send.at[i],
                    two_recv.at[i],
                    tp=chip,
                )

    def add_chip(k, h):
        two_copies[k, h].wait_recv()
        i = 2 * k + h
        total = (kept[k, h] + from_chip[k, h].astype(F32)).astype(BF16)
        if k == 0:
            home[part_rows(s, h), :] = total
        else:
            to_home[k, h] = total
            home_copies[k, h] = send(
                to_home.at[k, h],
                home.at[part_rows(s, h), :],
                home_send.at[i],
                home_recv.at[i],
                sp=sp_of[k],
            )

    stages = dict(F=forward, P=pass_on, C=experts, A=add_core, B=add_chip)
    order = (
        "F10 P00 F11 P01",
        "C0 F20 P10 F21",
        "P11 C1 F30 P20",
        "F31 P21 A10 A11",
        "C2 P30 P31 A20",
        "A21 B10 B11 C3",
        "A30 A31 B20 B21",
        "A00 A01 B30 B31",
        "B00 B01",
    )
    for line_of in order:
        for stage in line_of.split():
            stages[stage[0]](*map(int, stage[1:]))

    def finish(n, carry):
        cols = column(n)
        out[:, cols] = (stream[:, cols] + dot(back, home[:, cols])).astype(BF16)
        return carry

    for copy in home_copies.values():
        copy.wait_recv()
    lax.fori_loop(0, tiles, finish, 0)
    for copy in pending:
        copy.wait_send()


def fused(*args):
    (conv_input, _, _, _, out_proj, residual, gain, _, _, w_gate, w_up, w_down) = args
    rows, width = residual.shape
    count, channels = conv_input.shape
    local, _, units = w_gate.shape
    cap = rows // GROUPS
    w_down = w_down.reshape(local * units, width)
    args = args[:6] + (gain.reshape(1, width), args[7].T, args[8].T) + args[9:11] + (w_down,)
    vmem = pl.BlockSpec(memory_space=pltpu.VMEM)
    far = pl.BlockSpec(memory_space=pl.ANY)
    sems = pltpu.SemaphoreType.DMA
    return pl.pallas_call(
        fused_kernel,
        out_shape=jax.ShapeDtypeStruct((rows, width), BF16),
        in_specs=[far] * 3 + [vmem] + [far] * 2 + [vmem] * 3 + [far] * 3,
        out_specs=vmem,
        scratch_shapes=[
            pltpu.VMEM((count, channels), BF16),
            pltpu.VMEM((count, channels), BF16),
            pltpu.VMEM((count, channels), BF16),
            pltpu.VMEM((rows, width), BF16),
            pltpu.VMEM(out_proj.shape, BF16),
            pltpu.VMEM(w_gate.shape, BF16),
            pltpu.VMEM(w_up.shape, BF16),
            pltpu.VMEM(w_down.shape, BF16),
            pltpu.VMEM((2, 16, channels), BF16),
            pltpu.VMEM((count + 8, channels), F32),
            pltpu.VMEM((3, rows, channels), BF16),
            pltpu.VMEM((4, rows, channels), BF16),
            pltpu.VMEM((rows, width), F32),
            pltpu.VMEM((rows, width + LANES), BF16),
            pltpu.VMEM((4, 2, 2 * cap, width + LANES), BF16),
            pltpu.VMEM((4 * cap, local * units), BF16),
            pltpu.VMEM((4, 2, 2 * cap, width), BF16),
            pltpu.VMEM((4, 2, cap, width), BF16),
            pltpu.VMEM((4, 2, cap // 2, width), F32),
            pltpu.VMEM((4, 2, cap // 2, width), BF16),
            pltpu.VMEM((4, 2, cap // 2, width), BF16),
            pltpu.VMEM((4, 2, cap // 2, width), BF16),
            pltpu.VMEM((rows, width), BF16),
            sems((8,)),
            sems((2,)),
            sems((2,)),
            sems((3,)),
            sems((4,)),
        ]
        + [sems((8,))] * 14,
        compiler_params=pltpu.CompilerParams(
            collective_id=0, has_side_effects=True, vmem_limit_bytes=56 << 20
        ),
    )(*args)


def on_device(*args):
    residual, routes, w_gate = args[5], args[7], args[9]
    rows, local, seq_ranks = residual.shape[0], w_gate.shape[0], lax.axis_size("sp")
    dense = local == routes.shape[1] == 2 and local * seq_ranks == local * GROUPS
    if dense and lax.axis_size("tp") == 4 and rows % LANES == 0:
        return fused(*args)
    return generic(*args)


def solution(mesh):
    return jax.shard_map(
        on_device,
        mesh=mesh,
        in_specs=(
            P(("grp", "sp"), "tp"),
            P(("grp", "sp"), "tp"),
            P(("grp", "sp"), "tp"),
            P(),
            P(),
            P(("grp", "sp", "tp"), None),
            P(),
            P(("grp", "sp", "tp"), None),
            P(("grp", "sp", "tp"), None),
            P("sp", None, "tp"),
            P("sp", None, "tp"),
            P("sp", "tp", None),
        ),
        out_specs=P(("grp", "sp", "tp"), None),
        check_vma=False,
    )
```

profile of v0, /device:TPU:0, one launch (start us, length us, event | category | flops | bytes accessed | tf_op | source)
XLA Modules:
  0.0 53.0 jit_solution(18071964644717555575)
XLA Ops:
  0.0 51.1 %shard_map.118 = bf16[128,2048]{1,0:T(8,128)(2,1)} custom-call(bf16[512,256]{1,0:T(8,128)(2,1)} %input_hbm.1, bf16[512,256]{1,0:T(8,128)(2,1)} %pre_hbm.1, bf16[512,256]{1,0:T(8,128)(2,1)} %post_hbm.1, f32[3,1024]{1,0:T(4,128)} %conv_taps.1, bf16[1024,2048]{1,0:T(8,128)(2,1)} %proj_hbm.1, bf16[128,2048]{1,0:T(8,128)(2,1)} %residual_hbm.1, ...), custom_call_target="tpu_custom_call" | custom-call | tf_op jit(solution)/shard_map/pallas_call | solution.py:476
  51.1 1.9 %copy.14 = bf16[128,2048]{1,0:T(8,128)(2,1)} copy(bf16[128,2048]{1,0:T(8,128)(2,1)} %shard_map.118) | data formatting | bytes 1048576
where the time goes:
time: 53.3 us; the launch traced here: 53 us
  Pallas kernels  51.1 us (96%)
  local copies, waits for them, and re-layouts  1.88 us (4%)
    pallas_call x1, Pallas kernels, fused(): pl.pallas_call(fused_kernel, out_shape=jax.ShapeDtypeStruct((rows, width)...  51.1 us
    unnamed x1, local copies, waits for them, and re-layouts  1.88 us

commit v1 on v0

v1 whole, which is shorter than its diff:
```python
import functools

import jax
import jax.numpy as jnp
from jax import lax
from jax.experimental import pallas as pl
from jax.experimental.pallas import tpu as pltpu
from jax.sharding import PartitionSpec as P

GROUPS = 4
LANES = 128
F32, BF16 = jnp.float32, jnp.bfloat16


def shifted(block, axis, distance):
    devices = range(lax.axis_size(axis))
    route = [(i - distance, i) for i in devices if i - distance in devices]
    return lax.ppermute(block, axis, route)


def generic(
    conv_input,
    pre_gate,
    post_gate,
    conv_taps,
    out_proj,
    residual_in,
    norm_gain,
    routes,
    route_weight,
    w_gate,
    w_up,
    w_down,
):
    shards = lax.axis_size("tp")
    place = lax.axis_index("tp")
    seq_ranks = lax.axis_size("sp")
    channels = conv_input.shape[1]
    width = residual_in.shape[1]
    taps = lax.dynamic_slice_in_dim(conv_taps, place * channels, channels, 1)
    prior_input, prior_gate = shifted((conv_input[-2:], pre_gate[-2:]), "sp", 1)
    gated = jnp.concatenate(
        [
            prior_gate.astype(jnp.float32) * prior_input.astype(jnp.float32),
            pre_gate.astype(jnp.float32) * conv_input.astype(jnp.float32),
        ],
        axis=0,
    )
    conv = gated[2:] * taps[2] + gated[1:-1] * taps[1] + gated[:-2] * taps[0]
    mixed = (post_gate.astype(jnp.float32) * conv).astype(jnp.bfloat16)
    token_rows = lax.all_to_all(mixed, "tp", split_axis=0, concat_axis=1, tiled=True)
    projected = jnp.dot(token_rows, out_proj, preferred_element_type=jnp.float32)
    stream = residual_in.astype(jnp.float32) + projected
    scale = lax.rsqrt(jnp.mean(stream * stream, axis=-1, keepdims=True) + 1e-06)
    normed = (stream * scale * norm_gain).astype(jnp.bfloat16)
    block_rows = routes.shape[0]
    local_experts = w_gate.shape[0]
    experts = local_experts * seq_ranks
    capacity = 2 * block_rows // experts
    flat_routes = routes.reshape(-1)
    position = jnp.arange(flat_routes.shape[0], dtype=jnp.int32)
    earlier = (flat_routes[:, None] == flat_routes[None, :]) & (
        position[None, :] < position[:, None]
    )
    rank = jnp.sum(earlier.astype(jnp.int32), axis=1)
    slot = flat_routes * capacity + rank
    outgoing = (
        jnp.zeros((experts * capacity, width), jnp.bfloat16).at[slot].set(normed[position // 2])
    )
    outgoing = outgoing.reshape(seq_ranks, local_experts, capacity, width)
    spread = lax.all_gather(
        lax.all_to_all(outgoing, "sp", split_axis=0, concat_axis=0, tiled=True)[:, None],
        "tp",
        axis=1,
        tiled=True,
    )
    count = spread.shape[3]
    partials = []
    for expert in range(local_experts):
        rows = spread[:, :, expert].reshape(seq_ranks * shards * count, width)
        gate = jnp.dot(rows, w_gate[expert], preferred_element_type=jnp.float32)
        upper = jnp.dot(rows, w_up[expert], preferred_element_type=jnp.float32)
        hidden = (jax.nn.silu(gate) * upper).astype(jnp.bfloat16)
        part = jnp.dot(hidden, w_down[expert], preferred_element_type=jnp.float32).astype(
            jnp.bfloat16
        )
        partials.append(part.reshape(seq_ranks, shards, count, width))
    stacked = jnp.stack(partials, axis=2)
    summed = lax.psum_scatter(stacked, "tp", scatter_dimension=1, tiled=True).astype(jnp.float32)
    returned = lax.all_to_all(
        summed[:, 0].astype(jnp.bfloat16), "sp", split_axis=0, concat_axis=0, tiled=True
    )
    results = returned.reshape(experts * capacity, width)[slot]
    results = results.reshape(block_rows, 2, width).astype(jnp.float32)
    weighted = jnp.sum(route_weight[:, :, None] * results, axis=1)
    return (stream + weighted).astype(jnp.bfloat16)


def dot(a, b):
    return jnp.dot(a, b, preferred_element_type=F32)


ORDER = (
    "P00 F10 E00 P01",
    "F11 E01 A00 F20",
    "P10 E10 F21 P11",
    "E11 A10 A11 F30",
    "P20 E20 F31 P21",
    "E21 A20 A21 B10",
    "P30 E30 B11 P31",
    "E31 A30 A31 B20",
    "B21 A01 B30 B31",
    "B00 B01",
)


def fused_kernel(
    input_hbm,
    pre_hbm,
    post_hbm,
    taps_hbm,
    proj_hbm,
    residual_hbm,
    gain_hbm,
    routes_hbm,
    weight_hbm,
    gate_hbm,
    up_hbm,
    down_hbm,
    out,
    conv_input,
    pre_gate,
    post_gate,
    conv_taps,
    proj,
    residual,
    gain,
    routes,
    route_weight,
    w_gate,
    w_up,
    w_down,
    halo,
    gated,
    mix_out,
    mix_in,
    stream,
    weigh_out,
    weigh,
    leaving,
    tok,
    begun,
    hidden,
    part,
    from_core,
    kept,
    to_chip,
    from_chip,
    to_home,
    home,
    known,
    load_sem,
    sent,
    halo_recv,
    mix_recv,
    weigh_recv,
    z_recv,
    x_recv,
    core_recv,
    one_recv,
    two_recv,
    home_recv,
):
    s, t = lax.axis_index("sp"), lax.axis_index("tp")
    rows, width = residual.shape
    half = width // 2
    channels = conv_input.shape[1]
    cap = rows // GROUPS
    units = w_gate.shape[2]
    core, chip, far = t + 1 - 2 * (t % 2), (t + 2) % 4, 3 - t
    sp_of = [s, s + 1 - 2 * (s % 2), (s + 2) % 4, 3 - s]
    pos = lambda place: (place % 2) * 2 + place // 2
    middle = (s == 1) | (s == 2)
    X_SENT, Z_SENT, ONE_SENT, TWO_SENT, MIX_SENT, WEIGH_SENT, HALO_SENT = range(7)

    def describe(src, dst, group, recv_sem, **where):
        return pltpu.make_async_remote_copy(
            src_ref=src,
            dst_ref=dst,
            send_sem=sent.at[group],
            recv_sem=recv_sem,
            device_id=where,
            device_id_type=pl.DeviceIdType.MESH,
        )

    def send(*refs, **where):
        describe(*refs, **where).start()

    def wait_for(piece, sem):
        pltpu.make_async_copy(piece, piece, sem).wait()

    def signal(sem, **where):
        pl.semaphore_signal(sem, inc=1, device_id=where, device_id_type=pl.DeviceIdType.MESH)

    barrier = pltpu.get_barrier_semaphore()
    signal(barrier, sp=sp_of[1])

    @pl.when(middle)
    def _():
        signal(barrier, sp=sp_of[3])

    for other in (core, chip, far):
        signal(barrier, tp=other)
    loads = []
    for i, (a, b) in enumerate(
        (
            (input_hbm, conv_input),
            (pre_hbm, pre_gate),
            (post_hbm, post_gate),
            (taps_hbm, conv_taps),
            (routes_hbm, routes),
            (weight_hbm, route_weight),
            (gain_hbm, gain),
            (residual_hbm, residual),
            (proj_hbm, proj),
            (gate_hbm, w_gate),
            (up_hbm, w_up),
            (down_hbm, w_down),
        )
    ):
        loads.append(pltpu.make_async_copy(a, b, load_sem.at[i]))
    for load in loads[:7]:
        load.start()
    for load in loads[:4]:
        load.wait()
    for load in loads[7:]:
        load.start()

    count = conv_input.shape[0]
    gated[pl.ds(8, count), :] = pre_gate[...].astype(F32) * conv_input[...].astype(F32)
    taps = conv_taps[:, pl.ds(pl.multiple_of(t * channels, channels), channels)]

    def mix(place, low, size):
        start = pl.multiple_of(place * rows, rows) + low
        g = gated[pl.ds(start, size + 8), :]
        conv = g[8:] * taps[2:3] + g[7:-1] * taps[1:2] + g[6:-2] * taps[0:1]
        return (post_gate[pl.ds(start, size), :].astype(F32) * conv).astype(BF16)

    edge = 16
    partners = (chip, far, core)

    def send_mixed(i, low, size):
        piece = pl.ds(low, size)
        send(
            mix_out.at[i, piece, :],
            mix_in.at[t, piece, :],
            MIX_SENT,
            mix_recv.at[t],
            tp=partners[i],
        )

    def wait_mixed(place):
        wait_for(mix_in.at[place], mix_recv.at[place])

    gated[0:8, :] = jnp.zeros((8, channels), F32)
    for i in range(3):
        mix_out[i] = mix(partners[i], 0, rows)

    @pl.when(middle)
    def _():
        pl.semaphore_wait(barrier, 5)

    @pl.when(jnp.logical_not(middle))
    def _():
        pl.semaphore_wait(barrier, 4)

    def halo_copy(i):
        ref = (conv_input, pre_gate)[i]
        return describe(
            ref.at[pl.ds(count - 16, 16), :],
            halo.at[i],
            HALO_SENT,
            halo_recv.at[0],
            sp=(s + 1) % 4,
        )

    @pl.when(s < 3)
    def _():
        for i in range(2):
            halo_copy(i).start()

    for i in range(3):

        @pl.when(partners[i] > 0)
        def _():
            send_mixed(i, 0, rows)

        @pl.when(partners[i] == 0)
        def _():
            send_mixed(i, edge, rows - edge)

    @pl.when(middle)
    def _():
        signal(known, sp=sp_of[3])
        signal(known, sp=sp_of[1])

    for load in loads[4:6]:
        load.wait()
    first, second = routes[0:1, :], routes[1:2, :]
    epg = w_gate.shape[0]
    down = lax.broadcasted_iota(jnp.int32, (rows, rows), 0)
    across = lax.broadcasted_iota(jnp.int32, (rows, rows), 1)
    group = lax.broadcasted_iota(jnp.int32, (16, rows), 0)
    member = (first >= group * epg) & (first < group * epg + epg) & (group < GROUPS)
    member = jnp.where(member, 1.0, 0.0)
    earlier = jnp.where(down < across, 1.0, 0.0).astype(BF16)
    rank = dot(member.astype(BF16), earlier)
    slot = jnp.sum(member * (rank + (group * cap).astype(F32)), axis=0, keepdims=True)
    pick = jnp.where(slot == down.astype(F32), 1.0, 0.0)
    back = pick.T.astype(BF16)
    pick = pick.astype(BF16)
    low = jnp.where(first < second, route_weight[0:1, :], route_weight[1:2, :])
    high = jnp.where(first < second, route_weight[1:2, :], route_weight[0:1, :])
    low_top, high_top = low.astype(BF16).astype(F32), high.astype(BF16).astype(F32)
    line = lax.broadcasted_iota(jnp.int32, (LANES, rows), 0)
    scales = jnp.where(
        line == 0,
        low_top,
        jnp.where(
            line == 1,
            low - low_top,
            jnp.where(line == 2, high_top, jnp.where(line == 3, high - high_top, 0.0)),
        ),
    ).astype(BF16)
    scales = lax.dot_general(
        pick, scales, (((1,), (1,)), ((), ())), preferred_element_type=F32
    )
    weigh_out[...] = scales.astype(BF16)

    @pl.when(s > 0)
    def _():
        wait_for(halo, halo_recv.at[0])
        gated[0:8, :] = halo[0, 8:16, :].astype(F32) * halo[1, 8:16, :].astype(F32)

    for i in range(3):

        @pl.when(partners[i] == 0)
        def _():
            mix_out[i, 0:edge, :] = mix(0, 0, edge)
            send_mixed(i, 0, edge)

    mix_in[t] = mix(t, 0, rows)

    @pl.when(middle)
    def _():
        pl.semaphore_wait(known, 1)
        signal(known, sp=sp_of[1])

    @pl.when(jnp.logical_not(middle))
    def _():
        pl.semaphore_wait(known, 2)

    group_rows = lambda g: pl.ds(pl.multiple_of(g * cap, cap), cap)
    block = lambda place: pl.ds(pl.multiple_of(pos(place) * cap, cap), cap)
    for k in (1, 2, 3):
        send(
            weigh_out.at[group_rows(sp_of[k]), :],
            weigh.at[s, block(t), :],
            WEIGH_SENT,
            weigh_recv.at[0],
            sp=sp_of[k],
        )
    weigh[s, block(t), :] = weigh_out[group_rows(s), :]

    def forward_weigh():
        wait_for(weigh.at[0:3, 0:cap, :], weigh_recv.at[0])
        for k in range(4):
            mine = weigh.at[sp_of[k], block(t), :]
            src = mine if k else weigh_out.at[group_rows(s), :]
            send(src, mine, WEIGH_SENT, weigh_recv.at[1], tp=chip)
            send(src, mine, WEIGH_SENT, weigh_recv.at[2], tp=core)

    def pass_weigh():
        wait_for(weigh.at[:, 0:cap, :], weigh_recv.at[1])
        for k in range(4):
            arrived = weigh.at[sp_of[k], block(chip), :]
            send(arrived, arrived, WEIGH_SENT, weigh_recv.at[2], tp=core)

    tile = 512
    tiles = width // tile
    column = lambda n: pl.ds(pl.multiple_of(n * tile, tile), tile)
    weights_of = lambda place: pl.ds(pl.multiple_of(place * channels, channels), channels)
    loads[7].wait()
    loads[8].wait()
    wait_mixed(core)

    def project_near(n, carry):
        cols = column(n)
        total = residual[:, cols].astype(F32)
        for place in (t, core):
            total += dot(mix_in[place], proj[weights_of(place), cols])
        stream[:, cols] = total
        return carry

    lax.fori_loop(0, tiles, project_near, 0)
    wait_mixed(chip)

    def project_chip(n, carry):
        cols = column(n)
        stream[:, cols] += dot(mix_in[chip], proj[weights_of(chip), cols])
        return carry

    lax.fori_loop(0, tiles, project_chip, 0)
    forward_weigh()
    wait_mixed(far)

    def project_far(n, squares):
        cols = column(n)
        total = stream[:, cols] + dot(mix_in[far], proj[weights_of(far), cols])
        stream[:, cols] = total
        return squares + jnp.sum(total * total, axis=1, keepdims=True)

    squares = lax.fori_loop(0, tiles, project_far, jnp.zeros((rows, 1), F32))
    scale = lax.rsqrt(squares / width + 1e-06)
    loads[6].wait()

    def forward(k, h):
        dst = tok.at[sp_of[k], h, block(t), :]
        src = leaving.at[h, group_rows(s), :]
        if k:
            wait_for(dst, z_recv.at[2 * k + h - 2])
            src = dst
        i = 2 * k + h
        send(src, dst, X_SENT, x_recv.at[i], tp=chip)
        send(src, dst, X_SENT, core_recv.at[i], tp=core)
        if not k:
            tok[s, h, block(t), :] = leaving[h, group_rows(s), :]

    def leave(k, h):
        send(
            leaving.at[h, group_rows(sp_of[k]), :],
            tok.at[s, h, block(t), :],
            Z_SENT,
            z_recv.at[2 * k + h - 2],
            sp=sp_of[k],
        )

    for h in (0, 1):

        def norm(n, carry):
            cols = column(n + h * (tiles // 2))
            row = (stream[:, cols] * scale * gain[:, cols]).astype(BF16)
            leaving[h, :, column(n)] = dot(pick, row).astype(BF16)
            return carry

        lax.fori_loop(0, tiles // 2, norm, 0)
        if h == 0:
            leave(1, 0)
            forward(0, 0)
    for k, h in ((1, 1), (2, 0), (2, 1), (3, 0), (3, 1)):
        leave(k, h)
    forward(0, 1)
    pass_weigh()
    for load in loads[9:]:
        load.wait()

    def pass_on(k, h):
        i = 2 * k + h
        arrived = tok.at[sp_of[k], h, block(chip), :]
        wait_for(arrived, x_recv.at[i])
        send(arrived, arrived, X_SENT, core_recv.at[i], tp=core)

    weighed = []
    core_rows = lambda c: pl.ds(pl.multiple_of(c * 2 * cap, cap), 2 * cap)

    def experts(k, h):
        g = sp_of[k]
        wait_for(tok.at[g, h, 0 : 2 * cap, :], core_recv.at[2 * k + h])
        x = tok[g, h]
        deep = pl.ds(h * half, half)
        if h == 0:
            for e in range(epg):
                begun[2 * e] = dot(x, w_gate[e, deep, :])
                begun[2 * e + 1] = dot(x, w_up[e, deep, :])
            return
        if not weighed:
            wait_for(weigh.at[:, 0 : 2 * cap, :], weigh_recv.at[2])
            weighed.append(True)
        top = weigh[g].astype(F32)
        for e in range(epg):
            w = top[:, 2 * e : 2 * e + 1] + top[:, 2 * e + 1 : 2 * e + 2]
            gate = begun[2 * e] + dot(x, w_gate[e, deep, :])
            upper = begun[2 * e + 1] + dot(x, w_up[e, deep, :])
            act = gate / (1.0 + jnp.exp(-gate)) * upper * w
            hidden[:, pl.ds(e * units, units)] = act.astype(BF16)
        for h in (0, 1):

            def lower(n, carry):
                cols = column(n + h * (tiles // 2))
                part[k, h, :, column(n)] = dot(hidden[...], w_down[:, cols]).astype(BF16)
                return carry

            lax.fori_loop(0, tiles // 2, lower, 0)
            i = 2 * k + h
            send(
                part.at[k, h, core_rows(1 - t % 2), :],
                from_core.at[k, h],
                ONE_SENT,
                one_recv.at[i],
                tp=core,
            )

    def add_core(k, h):
        i = 2 * k + h
        wait_for(from_core.at[k, h], one_recv.at[i])
        for mine in (False, True):
            x = t // 2 if mine else 1 - t // 2
            base = pl.multiple_of((t % 2) * 2 * cap + x * cap, cap)
            near = pl.multiple_of(x * cap, cap)
            total = part[k, h, pl.ds(base, cap), :].astype(F32)
            total += from_core[k, h, pl.ds(near, cap), :].astype(F32)
            if mine:
                kept[k, h] = total
            else:
                to_chip[k, h] = total.astype(BF16)
                send(
                    to_chip.at[k, h],
                    from_chip.at[k, h],
                    TWO_SENT,
                    two_recv.at[i],
                    tp=chip,
                )

    def add_chip(k, h):
        wait_for(from_chip.at[k, h], two_recv.at[2 * k + h])
        total = (kept[k, h] + from_chip[k, h].astype(F32)).astype(BF16)
        if k == 0:
            home[h, group_rows(s), :] = total
        else:
            to_home[k, h] = total
            send(
                to_home.at[k, h],
                home.at[h, group_rows(s), :],
                Z_SENT,
                home_recv.at[h],
                sp=sp_of[k],
            )

    stages = dict(F=forward, P=pass_on, E=experts, A=add_core, B=add_chip)
    for line_of in ORDER:
        for stage in line_of.split():
            stages[stage[0]](*map(int, stage[1:]))

    for h in (0, 1):

        def finish(n, carry):
            cols = column(n + h * (tiles // 2))
            out[:, cols] = (stream[:, cols] + dot(back, home[h, :, column(n)])).astype(BF16)
            return carry

        wait_for(home.at[h, 0 : 3 * cap, :], home_recv.at[h])
        lax.fori_loop(0, tiles // 2, finish, 0)
    wait_for(tok.at[0:3], sent.at[X_SENT])
    wait_for(tok.at[0:3, :, 0 : 2 * cap, :], sent.at[Z_SENT])
    wait_for(tok.at[0:2], sent.at[ONE_SENT])
    wait_for(tok.at[0], sent.at[TWO_SENT])
    wait_for(mix_out, sent.at[MIX_SENT])
    wait_for(weigh.at[0:3], sent.at[WEIGH_SENT])
    wait_for(weigh.at[0:3, 0:cap, :], sent.at[WEIGH_SENT])

    @pl.when(s < 3)
    def _():
        wait_for(halo, sent.at[HALO_SENT])


def fused(*args):
    (conv_input, _, _, _, out_proj, residual, gain, _, _, w_gate, w_up, w_down) = args
    rows, width = residual.shape
    count, channels = conv_input.shape
    local, _, units = w_gate.shape
    cap = rows // GROUPS
    half = width // 2
    w_down = w_down.reshape(local * units, width)
    args = args[:6] + (gain.reshape(1, width), args[7].T, args[8].T) + args[9:11] + (w_down,)
    far = pl.BlockSpec(memory_space=pl.ANY)
    vmem, sems = pltpu.VMEM, pltpu.SemaphoreType.DMA
    return pl.pallas_call(
        fused_kernel,
        out_shape=vmem((rows, width), BF16),
        in_specs=[far] * 12,
        out_specs=pl.BlockSpec(memory_space=vmem),
        scratch_shapes=[vmem(arg.shape, arg.dtype) for arg in args]
        + [
            vmem((2, 16, channels), BF16),
            vmem((count + 8, channels), F32),
            vmem((3, rows, channels), BF16),
            vmem((4, rows, channels), BF16),
            vmem((rows, width), F32),
            vmem((rows, LANES), BF16),
            vmem((4, rows, LANES), BF16),
            vmem((2, rows, half), BF16),
            vmem((4, 2, rows, half), BF16),
            vmem((2 * local, rows, units), F32),
            vmem((rows, local * units), BF16),
            vmem((4, 2, rows, half), BF16),
            vmem((4, 2, 2 * cap, half), BF16),
            vmem((4, 2, cap, half), F32),
            vmem((4, 2, cap, half), BF16),
            vmem((4, 2, cap, half), BF16),
            vmem((4, 2, cap, half), BF16),
            vmem((2, rows, half), BF16),
            pltpu.SemaphoreType.REGULAR,
        ]
        + [sems((n,)) for n in (12, 7, 1, 4, 3, 6, 8, 8, 8, 8, 2)],
        compiler_params=pltpu.CompilerParams(
            collective_id=0, has_side_effects=True, vmem_limit_bytes=56 << 20
        ),
    )(*args)


def on_device(*args):
    residual, routes, w_gate = args[5], args[7], args[9]
    rows, local, seq_ranks = residual.shape[0], w_gate.shape[0], lax.axis_size("sp")
    dense = local == routes.shape[1] == 2 and local * seq_ranks == local * GROUPS
    if dense and lax.axis_size("tp") == 4 and rows % LANES == 0:
        return fused(*args)
    return generic(*args)


def solution(mesh):
    return jax.shard_map(
        on_device,
        mesh=mesh,
        in_specs=(
            P(("grp", "sp"), "tp"),
            P(("grp", "sp"), "tp"),
            P(("grp", "sp"), "tp"),
            P(),
            P(),
            P(("grp", "sp", "tp"), None),
            P(),
            P(("grp", "sp", "tp"), None),
            P(("grp", "sp", "tp"), None),
            P("sp", None, "tp"),
            P("sp", None, "tp"),
            P("sp", "tp", None),
        ),
        out_specs=P(("grp", "sp", "tp"), None),
        check_vma=False,
    )
```

time: 53.3 us -> 49.8 us (0.934)
  Pallas kernels: 51.1 us -> 48.9 us
  local copies, waits for them, and re-layouts: 1.88 us -> 0.8 us
    pallas_call x1, Pallas kernels: 51.1 us -> 48.9 us  [fused(): pl.pallas_call(fused_kernel, out_shape=vmem((rows, width), BF16), in_spec...]
    unnamed x1, local copies, waits for them, and re-layouts: 1.88 us -> 0.8 us
where the time goes in v1:
time: 49.8 us; the launch traced here: 49.7 us
  Pallas kernels  48.9 us (98%)
  local copies, waits for them, and re-layouts  0.8 us (2%)
    pallas_call x1, Pallas kernels, fused(): pl.pallas_call(fused_kernel, out_shape=vmem((rows, width), BF16), in_spec...  48.9 us

profile of v1, /device:TPU:0, one launch (start us, length us, event | category | flops | bytes accessed | tf_op | source)
XLA Modules:
  0.0 49.7 jit_solution(12898671511598859333)
XLA Ops:
  0.0 48.9 %shard_map.118 = bf16[128,2048]{1,0:T(8,128)(2,1)S(1)} custom-call(bf16[512,256]{1,0:T(8,128)(2,1)} %input_hbm.1, bf16[512,256]{1,0:T(8,128)(2,1)} %pre_hbm.1, bf16[512,256]{1,0:T(8,128)(2,1)} %post_hbm.1, f32[3,1024]{1,0:T(4,128)} %taps_hbm.1, bf16[1024,2048]{1,0:T(8,128)(2,1)} %proj_hbm.1, bf16[128,2048]{1,0:T(8,128)(2,1)} %residual_hbm.1, ...), custom_call_target="tpu_custom_call" | custom-call | tf_op jit(solution)/shard_map/pallas_call | solution.py:587
  48.9 0.8 %copy.14 = bf16[128,2048]{1,0:T(8,128)(2,1)} copy(bf16[128,2048]{1,0:T(8,128)(2,1)S(1)} %shard_map.118) | data formatting | bytes 1048576

commit v2 on v1

--- a/solution.py
+++ b/solution.py
@@ -100,18 +100,24 @@
     return jnp.dot(a, b, preferred_element_type=F32)
 
 
+EARLY = ("Z10 F00",)
 ORDER = (
-    "P00 F10 E00 P01",
-    "F11 E01 A00 F20",
-    "P10 E10 F21 P11",
-    "E11 A10 A11 F30",
-    "P20 E20 F31 P21",
-    "E21 A20 A21 B10",
-    "P30 E30 B11 P31",
-    "E31 A30 A31 B20",
-    "B21 A01 B30 B31",
-    "B00 B01",
+    "Z11 Z20 Z21 Z30",
+    "Z31 F01 W P00",
+    "F10 E00 V P01",
+    "F11 Y E01 L00",
+    "L01 A00 F20 P10",
+    "E10 F21 P11 E11",
+    "L10 L11 A10 A11",
+    "F30 P20 F31 P21",
+    "E20 E21 L20 L21",
+    "A20 A21 B10 P30",
+    "E30 A01 B11 P31",
+    "E31 L30 L31 A30",
+    "B20 B21 A31 B30",
+    "B00 B01 B31",
 )
+ORDERS = (ORDER, ORDER, ORDER, ORDER)
 
 
 def fused_kernel(
@@ -356,12 +362,54 @@
         pl.semaphore_wait(known, 1)
         signal(known, sp=sp_of[1])
 
-    @pl.when(jnp.logical_not(middle))
-    def _():
-        pl.semaphore_wait(known, 2)
-
     group_rows = lambda g: pl.ds(pl.multiple_of(g * cap, cap), cap)
     block = lambda place: pl.ds(pl.multiple_of(pos(place) * cap, cap), cap)
+    weigh[s, block(t), :] = weigh_out[group_rows(s), :]
+
+    def forward_weigh():
+        wait_for(weigh.at[0:3, 0:cap, :], weigh_recv.at[0])
+        for k in range(4):
+            mine = weigh.at[sp_of[k], block(t), :]
+            src = mine if k else weigh_out.at[group_rows(s), :]
+            send(src, mine, WEIGH_SENT, weigh_recv.at[1], tp=chip)
+            send(src, mine, WEIGH_SENT, weigh_recv.at[2], tp=core)
+
+    def pass_weigh():
+        wait_for(weigh.at[:, 0:cap, :], weigh_recv.at[1])
+        for k in range(4):
+            arrived = weigh.at[sp_of[k], block(chip), :]
+            send(arrived, arrived, WEIGH_SENT, weigh_recv.at[2], tp=core)
+
+    tile = 512
+    tiles = width // tile
+    column = lambda n: pl.ds(pl.multiple_of(n * tile, tile), tile)
+    weights_of = lambda place: pl.ds(pl.multiple_of(place * channels, channels), channels)
+    loads[7].wait()
+    loads[8].wait()
+    wait_mixed(core)
+
+    def project_near(n, carry):
+        cols = column(n)
+        total = residual[:, cols].astype(F32)
+        for place in (t, core):
+            total += dot(mix_in[place], proj[weights_of(place), cols])
+        stream[:, cols] = total
+        return carry
+
+    lax.fori_loop(0, tiles, project_near, 0)
+    wait_mixed(chip)
+
+    def project_chip(n, carry):
+        cols = column(n)
+        stream[:, cols] += dot(mix_in[chip], proj[weights_of(chip), cols])
+        return carry
+
+    lax.fori_loop(0, tiles, project_chip, 0)
+
+    @pl.when(jnp.logical_not(middle))
+    def _():
+        pl.semaphore_wait(known, 2)
+
     for k in (1, 2, 3):
         send(
             weigh_out.at[group_rows(sp_of[k]), :],
@@ -370,48 +418,6 @@
             weigh_recv.at[0],
             sp=sp_of[k],
         )
-    weigh[s, block(t), :] = weigh_out[group_rows(s), :]
-
-    def forward_weigh():
-        wait_for(weigh.at[0:3, 0:cap, :], weigh_recv.at[0])
-        for k in range(4):
-            mine = weigh.at[sp_of[k], block(t), :]
-            src = mine if k else weigh_out.at[group_rows(s), :]
-            send(src, mine, WEIGH_SENT, weigh_recv.at[1], tp=chip)
-            send(src, mine, WEIGH_SENT, weigh_recv.at[2], tp=core)
-
-    def pass_weigh():
-        wait_for(weigh.at[:, 0:cap, :], weigh_recv.at[1])
-        for k in range(4):
-            arrived = weigh.at[sp_of[k], block(chip), :]
-            send(arrived, arrived, WEIGH_SENT, weigh_recv.at[2], tp=core)
-
-    tile = 512
-    tiles = width // tile
-    column = lambda n: pl.ds(pl.multiple_of(n * tile, tile), tile)
-    weights_of = lambda place: pl.ds(pl.multiple_of(place * channels, channels), channels)
-    loads[7].wait()
-    loads[8].wait()
-    wait_mixed(core)
-
-    def project_near(n, carry):
-        cols = column(n)
-        total = residual[:, cols].astype(F32)
-        for place in (t, core):
-            total += dot(mix_in[place], proj[weights_of(place), cols])
-        stream[:, cols] = total
-        return carry
-
-    lax.fori_loop(0, tiles, project_near, 0)
-    wait_mixed(chip)
-
-    def project_chip(n, carry):
-        cols = column(n)
-        stream[:, cols] += dot(mix_in[chip], proj[weights_of(chip), cols])
-        return carry
-
-    lax.fori_loop(0, tiles, project_chip, 0)
-    forward_weigh()
     wait_mixed(far)
 
     def project_far(n, squares):
@@ -455,12 +461,9 @@
 
         lax.fori_loop(0, tiles // 2, norm, 0)
         if h == 0:
-            leave(1, 0)
-            forward(0, 0)
-    for k, h in ((1, 1), (2, 0), (2, 1), (3, 0), (3, 1)):
-        leave(k, h)
-    forward(0, 1)
-    pass_weigh()
+            for stage in " ".join(EARLY).split():
+                (leave if stage[0] == "Z" else forward)(*map(int, stage[1:]))
+
     for load in loads[9:]:
         load.wait()
 
@@ -470,7 +473,6 @@
         wait_for(arrived, x_recv.at[i])
         send(arrived, arrived, X_SENT, core_recv.at[i], tp=core)
 
-    weighed = []
     core_rows = lambda c: pl.ds(pl.multiple_of(c * 2 * cap, cap), 2 * cap)
 
     def experts(k, h):
@@ -480,35 +482,31 @@
         deep = pl.ds(h * half, half)
         if h == 0:
             for e in range(epg):
-                begun[2 * e] = dot(x, w_gate[e, deep, :])
-                begun[2 * e + 1] = dot(x, w_up[e, deep, :])
+                begun[k, 2 * e] = dot(x, w_gate[e, deep, :])
+                begun[k, 2 * e + 1] = dot(x, w_up[e, deep, :])
             return
-        if not weighed:
-            wait_for(weigh.at[:, 0 : 2 * cap, :], weigh_recv.at[2])
-            weighed.append(True)
         top = weigh[g].astype(F32)
         for e in range(epg):
             w = top[:, 2 * e : 2 * e + 1] + top[:, 2 * e + 1 : 2 * e + 2]
-            gate = begun[2 * e] + dot(x, w_gate[e, deep, :])
-            upper = begun[2 * e + 1] + dot(x, w_up[e, deep, :])
+            gate = begun[k, 2 * e] + dot(x, w_gate[e, deep, :])
+            upper = begun[k, 2 * e + 1] + dot(x, w_up[e, deep, :])
             act = gate / (1.0 + jnp.exp(-gate)) * upper * w
-            hidden[:, pl.ds(e * units, units)] = act.astype(BF16)
-        for h in (0, 1):
-
-            def lower(n, carry):
-                cols = column(n + h * (tiles // 2))
-                part[k, h, :, column(n)] = dot(hidden[...], w_down[:, cols]).astype(BF16)
-                return carry
-
-            lax.fori_loop(0, tiles // 2, lower, 0)
-            i = 2 * k + h
-            send(
-                part.at[k, h, core_rows(1 - t % 2), :],
-                from_core.at[k, h],
-                ONE_SENT,
-                one_recv.at[i],
-                tp=core,
-            )
+            hidden[k, :, pl.ds(e * units, units)] = act.astype(BF16)
+
+    def lower(k, h):
+        def step(n, carry):
+            cols = column(n + h * (tiles // 2))
+            part[k, h, :, column(n)] = dot(hidden[k], w_down[:, cols]).astype(BF16)
+            return carry
+
+        lax.fori_loop(0, tiles // 2, step, 0)
+        send(
+            part.at[k, h, core_rows(1 - t % 2), :],
+            from_core.at[k, h],
+            ONE_SENT,
+            one_recv.at[2 * k + h],
+            tp=core,
+        )
 
     def add_core(k, h):
         i = 2 * k + h
@@ -546,10 +544,30 @@
                 sp=sp_of[k],
             )
 
-    stages = dict(F=forward, P=pass_on, E=experts, A=add_core, B=add_chip)
-    for line_of in ORDER:
-        for stage in line_of.split():
-            stages[stage[0]](*map(int, stage[1:]))
+    stages = dict(
+        F=forward,
+        P=pass_on,
+        E=experts,
+        L=lower,
+        A=add_core,
+        B=add_chip,
+        W=forward_weigh,
+        V=pass_weigh,
+        Y=lambda: wait_for(weigh.at[:, 0 : 2 * cap, :], weigh_recv.at[2]),
+        Z=leave,
+    )
+    for order in dict.fromkeys(ORDERS):
+        where = [i for i in range(4) if ORDERS[i] == order]
+
+        def run():
+            for stage in " ".join(order).split():
+                stages[stage[0]](*map(int, stage[1:]))
+
+        if len(where) == 4:
+            run()
+        else:
+            chosen = functools.reduce(jnp.logical_or, [s == i for i in where])
+            pl.when(chosen)(run)
 
     for h in (0, 1):
 
@@ -600,8 +618,8 @@
             vmem((4, rows, LANES), BF16),
             vmem((2, rows, half), BF16),
             vmem((4, 2, rows, half), BF16),
-            vmem((2 * local, rows, units), F32),
-            vmem((rows, local * units), BF16),
+            vmem((4, 2 * local, rows, units), F32),
+            vmem((4, rows, local * units), BF16),
             vmem((4, 2, rows, half), BF16),
             vmem((4, 2, 2 * cap, half), BF16),
             vmem((4, 2, cap, half), F32),

time: 49.8 us -> 48.7 us (0.978)
  Pallas kernels: 48.9 us -> 47.7 us
    pallas_call x1, Pallas kernels: 48.9 us -> 47.7 us  [fused(): pl.pallas_call(fused_kernel, out_shape=vmem((rows, width), BF16), in_spec...]
where the time goes in v2:
time: 48.7 us; the launch traced here: 48.5 us
  Pallas kernels  47.7 us (98%)
  local copies, waits for them, and re-layouts  0.8 us (2%)
    pallas_call x1, Pallas kernels, fused(): pl.pallas_call(fused_kernel, out_shape=vmem((rows, width), BF16), in_spec...  47.7 us

profile of v2, /device:TPU:0, one launch (start us, length us, event | category | flops | bytes accessed | tf_op | source)
XLA Modules:
  0.0 48.5 jit_solution(9866010046406332936)
XLA Ops:
  0.0 47.7 %shard_map.118 = bf16[128,2048]{1,0:T(8,128)(2,1)S(1)} custom-call(bf16[512,256]{1,0:T(8,128)(2,1)} %input_hbm.1, bf16[512,256]{1,0:T(8,128)(2,1)} %pre_hbm.1, bf16[512,256]{1,0:T(8,128)(2,1)} %post_hbm.1, f32[3,1024]{1,0:T(4,128)} %taps_hbm.1, bf16[1024,2048]{1,0:T(8,128)(2,1)} %proj_hbm.1, bf16[128,2048]{1,0:T(8,128)(2,1)} %residual_hbm.1, ...), custom_call_target="tpu_custom_call" | custom-call | tf_op jit(solution)/shard_map/pallas_call | solution.py:605
  47.7 0.8 %copy.14 = bf16[128,2048]{1,0:T(8,128)(2,1)} copy(bf16[128,2048]{1,0:T(8,128)(2,1)S(1)} %shard_map.118) | data formatting | bytes 1048576

commit v3 on v2

--- a/solution.py
+++ b/solution.py
@@ -380,7 +380,7 @@
             arrived = weigh.at[sp_of[k], block(chip), :]
             send(arrived, arrived, WEIGH_SENT, weigh_recv.at[2], tp=core)
 
-    tile = 512
+    tile = 1024
     tiles = width // tile
     column = lambda n: pl.ds(pl.multiple_of(n * tile, tile), tile)
     weights_of = lambda place: pl.ds(pl.multiple_of(place * channels, channels), channels)

time: 48.7 us -> 47 us (0.965)
  Pallas kernels: 47.7 us -> 46 us
    pallas_call x1, Pallas kernels: 47.7 us -> 46 us  [fused(): pl.pallas_call(fused_kernel, out_shape=vmem((rows, width), BF16), in_spec...]
where the time goes in v3:
time: 47 us; the launch traced here: 46.8 us
  Pallas kernels  46 us (98%)
  local copies, waits for them, and re-layouts  0.8 us (2%)
    pallas_call x1, Pallas kernels, fused(): pl.pallas_call(fused_kernel, out_shape=vmem((rows, width), BF16), in_spec...  46 us

profile of v3, /device:TPU:0, one launch (start us, length us, event | category | flops | bytes accessed | tf_op | source)
XLA Modules:
  0.0 46.8 jit_solution(9097785849122454613)
XLA Ops:
  0.0 46.0 %shard_map.118 = bf16[128,2048]{1,0:T(8,128)(2,1)S(1)} custom-call(bf16[512,256]{1,0:T(8,128)(2,1)} %input_hbm.1, bf16[512,256]{1,0:T(8,128)(2,1)} %pre_hbm.1, bf16[512,256]{1,0:T(8,128)(2,1)} %post_hbm.1, f32[3,1024]{1,0:T(4,128)} %taps_hbm.1, bf16[1024,2048]{1,0:T(8,128)(2,1)} %proj_hbm.1, bf16[128,2048]{1,0:T(8,128)(2,1)} %residual_hbm.1, ...), custom_call_target="tpu_custom_call" | custom-call | tf_op jit(solution)/shard_map/pallas_call | solution.py:605
  46.0 0.8 %copy.14 = bf16[128,2048]{1,0:T(8,128)(2,1)} copy(bf16[128,2048]{1,0:T(8,128)(2,1)S(1)} %shard_map.118) | data formatting | bytes 1048576

commit v4 on v3

--- a/solution.py
+++ b/solution.py
@@ -106,16 +106,16 @@
     "Z31 F01 W P00",
     "F10 E00 V P01",
     "F11 Y E01 L00",
-    "L01 A00 F20 P10",
-    "E10 F21 P11 E11",
-    "L10 L11 A10 A11",
-    "F30 P20 F31 P21",
-    "E20 E21 L20 L21",
-    "A20 A21 B10 P30",
-    "E30 A01 B11 P31",
-    "E31 L30 L31 A30",
-    "B20 B21 A31 B30",
-    "B00 B01 B31",
+    "L01 F20 P10 E10",
+    "A00 F21 P11 E11",
+    "L10 L11 F30 P20",
+    "E20 F31 A10 P21",
+    "E21 P30 L20 L21",
+    "E30 A20 A21 P31",
+    "A11 E31 L30 L31",
+    "B10 B20 A30 A31",
+    "B21 A01 B11 B30",
+    "B31 B00 B01",
 )
 ORDERS = (ORDER, ORDER, ORDER, ORDER)
 
@@ -343,6 +343,31 @@
     )
     weigh_out[...] = scales.astype(BF16)
 
+    group_rows = lambda g: pl.ds(pl.multiple_of(g * cap, cap), cap)
+    block = lambda place: pl.ds(pl.multiple_of(pos(place) * cap, cap), cap)
+
+    def send_weigh(*others):
+        for k in others:
+            send(
+                weigh_out.at[group_rows(sp_of[k]), :],
+                weigh.at[s, block(t), :],
+                WEIGH_SENT,
+                weigh_recv.at[0],
+                sp=sp_of[k],
+            )
+
+    @pl.when(middle)
+    def _():
+        send_weigh(1, 3)
+        pl.semaphore_wait(known, 1)
+        signal(known, sp=sp_of[1])
+        send_weigh(2)
+
+    @pl.when(s == 3)
+    def _():
+        pl.semaphore_wait(known, 2)
+        send_weigh(1, 2, 3)
+
     @pl.when(s > 0)
     def _():
         wait_for(halo, halo_recv.at[0])
@@ -357,13 +382,7 @@
 
     mix_in[t] = mix(t, 0, rows)
 
-    @pl.when(middle)
-    def _():
-        pl.semaphore_wait(known, 1)
-        signal(known, sp=sp_of[1])
-
-    group_rows = lambda g: pl.ds(pl.multiple_of(g * cap, cap), cap)
-    block = lambda place: pl.ds(pl.multiple_of(pos(place) * cap, cap), cap)
+
     weigh[s, block(t), :] = weigh_out[group_rows(s), :]
 
     def forward_weigh():
@@ -397,6 +416,12 @@
         return carry
 
     lax.fori_loop(0, tiles, project_near, 0)
+
+    @pl.when(s == 0)
+    def _():
+        pl.semaphore_wait(known, 2)
+        send_weigh(1, 2, 3)
+
     wait_mixed(chip)
 
     def project_chip(n, carry):
@@ -405,19 +430,6 @@
         return carry
 
     lax.fori_loop(0, tiles, project_chip, 0)
-
-    @pl.when(jnp.logical_not(middle))
-    def _():
-        pl.semaphore_wait(known, 2)
-
-    for k in (1, 2, 3):
-        send(
-            weigh_out.at[group_rows(sp_of[k]), :],
-            weigh.at[s, block(t), :],
-            WEIGH_SENT,
-            weigh_recv.at[0],
-            sp=sp_of[k],
-        )
     wait_mixed(far)
 
     def project_far(n, squares):

time: 47 us -> 44.8 us (0.953)
  Pallas kernels: 46 us -> 43.8 us
    pallas_call x1, Pallas kernels: 46 us -> 43.8 us  [fused(): pl.pallas_call(fused_kernel, out_shape=vmem((rows, width), BF16), in_spec...]
where the time goes in v4:
time: 44.8 us; the launch traced here: 44.6 us
  Pallas kernels  43.8 us (98%)
  local copies, waits for them, and re-layouts  0.8 us (2%)
    pallas_call x1, Pallas kernels, fused(): pl.pallas_call(fused_kernel, out_shape=vmem((rows, width), BF16), in_spec...  43.8 us

profile of v4, /device:TPU:0, one launch (start us, length us, event | category | flops | bytes accessed | tf_op | source)
XLA Modules:
  0.0 44.6 jit_solution(9097868496903912850)
XLA Ops:
  0.0 43.8 %shard_map.118 = bf16[128,2048]{1,0:T(8,128)(2,1)S(1)} custom-call(bf16[512,256]{1,0:T(8,128)(2,1)} %input_hbm.1, bf16[512,256]{1,0:T(8,128)(2,1)} %pre_hbm.1, bf16[512,256]{1,0:T(8,128)(2,1)} %post_hbm.1, f32[3,1024]{1,0:T(4,128)} %taps_hbm.1, bf16[1024,2048]{1,0:T(8,128)(2,1)} %proj_hbm.1, bf16[128,2048]{1,0:T(8,128)(2,1)} %residual_hbm.1, ...), custom_call_target="tpu_custom_call" | custom-call | tf_op jit(solution)/shard_map/pallas_call | solution.py:617
  43.8 0.8 %copy.14 = bf16[128,2048]{1,0:T(8,128)(2,1)} copy(bf16[128,2048]{1,0:T(8,128)(2,1)S(1)} %shard_map.118) | data formatting | bytes 1048576

commit v5 on v4

--- a/solution.py
+++ b/solution.py
@@ -100,22 +100,22 @@
     return jnp.dot(a, b, preferred_element_type=F32)
 
 
-EARLY = ("Z10 F00",)
+EARLY = ("Z20 F00",)
 ORDER = (
-    "Z11 Z20 Z21 Z30",
+    "Z21 Z10 Z11 Z30",
     "Z31 F01 W P00",
-    "F10 E00 V P01",
-    "F11 Y E01 L00",
-    "L01 F20 P10 E10",
-    "A00 F21 P11 E11",
-    "L10 L11 F30 P20",
-    "E20 F31 A10 P21",
-    "E21 P30 L20 L21",
-    "E30 A20 A21 P31",
-    "A11 E31 L30 L31",
-    "B10 B20 A30 A31",
-    "B21 A01 B11 B30",
-    "B31 B00 B01",
+    "F20 E00 V P01",
+    "F21 Y E01 L00",
+    "L01 F10 P20 E20",
+    "A00 F11 P21 E21",
+    "L20 L21 F30 P10",
+    "E10 F31 A20 A21",
+    "P11 E11 P30 L10",
+    "L11 E30 P31 A10",
+    "E31 L30 L31 B20",
+    "B21 A30 A31 A11",
+    "B10 A01 B30 B31",
+    "B11 B00 B01",
 )
 ORDERS = (ORDER, ORDER, ORDER, ORDER)
 
@@ -422,23 +422,25 @@
         pl.semaphore_wait(known, 2)
         send_weigh(1, 2, 3)
 
-    wait_mixed(chip)
-
-    def project_chip(n, carry):
+    sooner = far + (t % 2) * (chip - far)
+    later = chip + far - sooner
+    wait_mixed(sooner)
+
+    def project_sooner(n, carry):
         cols = column(n)
-        stream[:, cols] += dot(mix_in[chip], proj[weights_of(chip), cols])
+        stream[:, cols] += dot(mix_in[sooner], proj[weights_of(sooner), cols])
         return carry
 
-    lax.fori_loop(0, tiles, project_chip, 0)
-    wait_mixed(far)
-
-    def project_far(n, squares):
+    lax.fori_loop(0, tiles, project_sooner, 0)
+    wait_mixed(later)
+
+    def project_later(n, squares):
         cols = column(n)
-        total = stream[:, cols] + dot(mix_in[far], proj[weights_of(far), cols])
+        total = stream[:, cols] + dot(mix_in[later], proj[weights_of(later), cols])
         stream[:, cols] = total
         return squares + jnp.sum(total * total, axis=1, keepdims=True)
 
-    squares = lax.fori_loop(0, tiles, project_far, jnp.zeros((rows, 1), F32))
+    squares = lax.fori_loop(0, tiles, project_later, jnp.zeros((rows, 1), F32))
     scale = lax.rsqrt(squares / width + 1e-06)
     loads[6].wait()
 

time: 44.8 us -> 44 us (0.982)
  Pallas kernels: 43.8 us -> 43.1 us
    pallas_call x1, Pallas kernels: 43.8 us -> 43.1 us  [fused(): pl.pallas_call(fused_kernel, out_shape=vmem((rows, width), BF16), in_spec...]
where the time goes in v5:
time: 44 us; the launch traced here: 43.9 us
  Pallas kernels  43.1 us (98%)
  local copies, waits for them, and re-layouts  0.8 us (2%)
    pallas_call x1, Pallas kernels, fused(): pl.pallas_call(fused_kernel, out_shape=vmem((rows, width), BF16), in_spec...  43.1 us

profile of v5, /device:TPU:0, one launch (start us, length us, event | category | flops | bytes accessed | tf_op | source)
XLA Modules:
  0.0 43.9 jit_solution(5106035559511186097)
XLA Ops:
  0.0 43.1 %shard_map.118 = bf16[128,2048]{1,0:T(8,128)(2,1)S(1)} custom-call(bf16[512,256]{1,0:T(8,128)(2,1)} %input_hbm.1, bf16[512,256]{1,0:T(8,128)(2,1)} %pre_hbm.1, bf16[512,256]{1,0:T(8,128)(2,1)} %post_hbm.1, f32[3,1024]{1,0:T(4,128)} %taps_hbm.1, bf16[1024,2048]{1,0:T(8,128)(2,1)} %proj_hbm.1, bf16[128,2048]{1,0:T(8,128)(2,1)} %residual_hbm.1, ...), custom_call_target="tpu_custom_call" | custom-call | tf_op jit(solution)/shard_map/pallas_call | solution.py:619
  43.1 0.8 %copy.14 = bf16[128,2048]{1,0:T(8,128)(2,1)} copy(bf16[128,2048]{1,0:T(8,128)(2,1)S(1)} %shard_map.118) | data formatting | bytes 1048576

commit v6 on v5

--- a/solution.py
+++ b/solution.py
@@ -112,8 +112,8 @@
     "E10 F31 A20 A21",
     "P11 E11 P30 L10",
     "L11 E30 P31 A10",
-    "E31 L30 L31 B20",
-    "B21 A30 A31 A11",
+    "A11 E31 L30 L31",
+    "B20 B21 A30 A31",
     "B10 A01 B30 B31",
     "B11 B00 B01",
 )

time: 44 us -> 43.6 us (level)
  Pallas kernels: 43.1 us -> 42.6 us
where the time goes in v6:
time: 43.6 us; the launch traced here: 43.4 us
  Pallas kernels  42.6 us (98%)
  local copies, waits for them, and re-layouts  0.8 us (2%)
    pallas_call x1, Pallas kernels, fused(): pl.pallas_call(fused_kernel, out_shape=vmem((rows, width), BF16), in_spec...  42.6 us

profile of v6, /device:TPU:0, one launch (start us, length us, event | category | flops | bytes accessed | tf_op | source)
XLA Modules:
  0.0 43.4 jit_solution(6070187478216103485)
XLA Ops:
  0.0 42.6 %shard_map.118 = bf16[128,2048]{1,0:T(8,128)(2,1)S(1)} custom-call(bf16[512,256]{1,0:T(8,128)(2,1)} %input_hbm.1, bf16[512,256]{1,0:T(8,128)(2,1)} %pre_hbm.1, bf16[512,256]{1,0:T(8,128)(2,1)} %post_hbm.1, f32[3,1024]{1,0:T(4,128)} %taps_hbm.1, bf16[1024,2048]{1,0:T(8,128)(2,1)} %proj_hbm.1, bf16[128,2048]{1,0:T(8,128)(2,1)} %residual_hbm.1, ...), custom_call_target="tpu_custom_call" | custom-call | tf_op jit(solution)/shard_map/pallas_call | solution.py:619
  42.7 0.8 %copy.14 = bf16[128,2048]{1,0:T(8,128)(2,1)} copy(bf16[128,2048]{1,0:T(8,128)(2,1)S(1)} %shard_map.118) | data formatting | bytes 1048576
